TPU v7x, 32 devices: a whole 2x2x4 slice. The times are simulated.
32 devices in a mesh: sp: 8 (over z, x), tp: 4 (over y, core).
Axes of the slice: x: 2, y: 2, z: 4, core: 2. Of those that a mesh axis runs over, the one named last changes fastest.
Arguments:
- residual: bfloat16 [2048, 2048], P(('sp', 'tp')), may hold values from -6 to 6
- first_query: bfloat16 [2048, 512], P('sp', 'tp'), may hold values from -6 to 6
- second_query: bfloat16 [2048, 512], P('sp', 'tp'), may hold values from -6 to 6
- first_key: bfloat16 [2048, 512], P('sp', 'tp'), may hold values from -6 to 6
- second_key: bfloat16 [2048, 512], P('sp', 'tp'), may hold values from -6 to 6
- values: bfloat16 [2048, 1024], P('sp', 'tp'), may hold values from -6 to 6
- lambdas: float32 [8], P('tp'), may hold values from 0.3 to 0.8
- head_gain: float32 [128], replicated, may hold values from 0.1 to 1.9
- out_weight: bfloat16 [1024, 2048], P('tp'), may hold values from -0.1875 to 0.1875
- norm_gain: float32 [2048], replicated, may hold values from 0.1 to 1.9
- up_weight: bfloat16 [2048, 4096], P('sp', 'tp'), may hold values from -0.125 to 0.125
- down_weight: bfloat16 [4096, 2048], P('tp', 'sp'), may hold values from -0.09375 to 0.09375
Outputs:
- mixed: bfloat16 [2048, 2048], P(('sp', 'tp'))
All inputs are finite; a program needn't handle non-finite values.
Results may differ from a plain program's by a relative error of at most 0.019.
Values may be sent and summed in bfloat16 or wider, within the bound.
A program may use at most 128 MiB of HBM per device.

v0:
```python
import jax
import jax.numpy as jnp
from jax import lax
from jax.sharding import PartitionSpec as P


def rotate(blocked, positions):
    half = blocked.shape[-1] // 2
    inverse = 10000.0 ** (-jnp.arange(0, half, dtype=jnp.float32) * 2.0 / blocked.shape[-1])
    angle = positions[:, None] * inverse[None, :]
    cosine = jnp.cos(angle)[:, None, :]
    sine = jnp.sin(angle)[:, None, :]
    first, second = (blocked[..., :half], blocked[..., half:])
    return jnp.concatenate(
        [first * cosine - second * sine, second * cosine + first * sine], axis=-1
    )


def absorb(state, queries, keys, vals, factor):
    top, total, summed = state
    scores = jnp.einsum("qhe,khe->qhk", queries, keys, preferred_element_type=jnp.float32) * factor
    peak = jnp.maximum(top, jnp.max(scores, axis=-1))
    shrink = jnp.exp(top - peak)
    weights = jnp.exp(scores - peak[..., None])
    total = total * shrink + jnp.sum(weights, axis=-1)
    summed = summed * shrink[..., None] + jnp.einsum(
        "qhk,khe->qhe", weights.astype(jnp.bfloat16), vals, preferred_element_type=jnp.float32
    )
    return (peak, total, summed)


def layer_norm(stream, gain):
    center = stream - jnp.mean(stream, axis=-1, keepdims=True)
    spread = jnp.mean(center * center, axis=-1, keepdims=True)
    return center * lax.rsqrt(spread + 1e-05) * gain


def local(
    residual,
    first_query,
    second_query,
    first_key,
    second_key,
    values,
    lambdas,
    head_gain,
    out_weight,
    norm_gain,
    up_weight,
    down_weight,
):
    local_rows = first_query.shape[0]
    head_count = lambdas.shape[0]
    head_width = first_query.shape[1] // head_count
    value_width = values.shape[1] // head_count
    quarter_rows = local_rows // lax.axis_size("tp")
    factor = head_width ** (-0.5)
    positions = (lax.axis_index("sp") * local_rows + jnp.arange(local_rows)).astype(jnp.float32)

    def prepare(source):
        turned = rotate(
            source.astype(jnp.float32).reshape(local_rows, head_count, head_width), positions
        )
        return turned.astype(jnp.bfloat16)

    query_a, query_b = (prepare(first_query), prepare(second_query))
    key_a = prepare(first_key).reshape(local_rows, head_count * head_width)
    key_b = prepare(second_key).reshape(local_rows, head_count * head_width)
    start_state = (
        jnp.full((local_rows, head_count), -1e30, jnp.float32),
        jnp.zeros((local_rows, head_count), jnp.float32),
        jnp.zeros((local_rows, head_count, value_width), jnp.float32),
    )
    piece_a = lax.all_gather(key_a, "sp", axis=0, tiled=True)
    piece_b = lax.all_gather(key_b, "sp", axis=0, tiled=True)
    piece_v = lax.all_gather(values, "sp", axis=0, tiled=True)
    count = piece_a.shape[0]
    block = 512
    blocks = count // block

    def advance(state, item):
        block_a, block_b, block_v = item
        return (
            (
                absorb(state[0], query_a, block_a, block_v, factor),
                absorb(state[1], query_b, block_b, block_v, factor),
            ),
            None,
        )

    items = (
        piece_a.reshape(blocks, block, head_count, head_width),
        piece_b.reshape(blocks, block, head_count, head_width),
        piece_v.reshape(blocks, block, head_count, value_width),
    )
    state_a, state_b = lax.scan(advance, (start_state, start_state), items)[0]
    diff = state_a[2] / state_a[1][..., None] - lambdas[None, :, None] * (
        state_b[2] / state_b[1][..., None]
    )
    scale = lax.rsqrt(jnp.mean(diff * diff, axis=-1, keepdims=True) + 1e-05)
    flat = (
        (diff * scale * head_gain * 0.8)
        .astype(jnp.bfloat16)
        .reshape(local_rows, head_count * value_width)
    )
    projected = lax.psum(
        jnp.dot(flat, out_weight, preferred_element_type=jnp.float32).astype(jnp.bfloat16), "tp"
    ).astype(jnp.float32)
    stream = lax.all_gather(residual, "tp", axis=0, tiled=True)
    whole = layer_norm(stream.astype(jnp.float32) + projected, norm_gain).astype(jnp.bfloat16)
    own_normed = lax.dynamic_slice_in_dim(
        whole, lax.axis_index("tp") * quarter_rows, quarter_rows, 0
    )
    lifted = jnp.dot(
        whole,
        lax.all_gather(up_weight, "sp", axis=0, tiled=True),
        preferred_element_type=jnp.float32,
    )
    down_full = lax.all_gather(down_weight, "sp", axis=1, tiled=True)
    hidden = jnp.square(jax.nn.relu(lifted)).astype(jnp.bfloat16)
    lowered = lax.psum_scatter(
        jnp.dot(hidden, down_full, preferred_element_type=jnp.float32).astype(jnp.bfloat16),
        "tp",
        scatter_dimension=0,
        tiled=True,
    ).astype(jnp.float32)
    return (own_normed.astype(jnp.float32) + lowered).astype(jnp.bfloat16)


def solution(mesh):
    in_specs = (
        P(("sp", "tp"), None),
        P("sp", "tp"),
        P("sp", "tp"),
        P("sp", "tp"),
        P("sp", "tp"),
        P("sp", "tp"),
        P("tp"),
        P(),
        P("tp", None),
        P(),
        P("sp", "tp"),
        P("tp", "sp"),
    )
    out_specs = P(("sp", "tp"), None)
    return jax.shard_map(local, mesh=mesh, in_specs=in_specs, out_specs=out_specs, check_vma=False)
```

profile of v0, /device:TPU:0, one launch (start us, length us, event | category | flops | bytes accessed | tf_op | source)
XLA Modules:
  0.0 354.3 jit_solution(2607594345238030326)
XLA Ops:
  12.2 34.2 %all_gather.21 = bf16[2048,128]{0,1:T(8,128)(2,1)S(1)} all-gather(bf16[256,128]{0,1:T(8,128)(2,1)S(1)} %bitcast.66), channel_id=1, replica_groups=mesh['sp'=8,'tp'=4] {'sp'}, dimensions={0}, use_global_device_ids=true | all-gather | bytes 589824 | tf_op jit(solution)/shard_map/all_gather | solution.py:75
  47.7 31.6 %all_gather.19 = bf16[2048,128]{0,1:T(8,128)(2,1)S(1)} all-gather(bf16[256,128]{0,1:T(8,128)(2,1)S(1)} %bitcast.67), channel_id=1, replica_groups=mesh['sp'=8,'tp'=4] {'sp'}, dimensions={0}, use_global_device_ids=true | all-gather | bytes 589824 | tf_op jit(solution)/shard_map/all_gather | solution.py:74
  80.6 2.1 reshape.134
  82.7 42.6 %while.21 = (s32[]{:T(128)}, f32[256,2]{0,1:T(2,128)S(1)}, f32[256,2]{0,1:T(2,128)}, f32[256,2,128]{0,2,1:T(8,128)}, f32[256,2]{0,1:T(2,128)S(1)}, /*index=5*/f3...) while((s32[]{:T(128)}, f32[256,2]{0,1:T(2,128)S(1)}, ...), condition=%wide.region_5.6_spmd.clone, body=%wide.region_0.5_spmd.clone.sunk | while | flops 204870656 | bytes 9381043 | solution.py:96
  82.7 1.3 fusion.60
  84.2 1.3 fusion.62
  86.3 1.8 constant_dynamic-slice_fusion.2
  89.2 1.7 fusion.68
  92.0 1.3 fusion.60
  93.4 1.3 fusion.62
  94.9 1.3 fusion.66
  96.2 1.8 constant_dynamic-slice_fusion.2
  99.1 2.0 fusion.68
  101.1 2.0 fusion.67
  104.5 1.3 fusion.62
  106.0 1.3 fusion.66
  107.3 1.8 constant_dynamic-slice_fusion.2
  110.2 2.0 fusion.68
  112.2 2.0 fusion.67
  115.7 1.3 fusion.62
  117.1 1.3 fusion.66
  118.4 1.8 constant_dynamic-slice_fusion.2
  121.4 2.0 fusion.68
  123.4 2.0 fusion.67
  127.3 1.4 convolution_convert_fusion.1
  130.0 35.5 %all-reduce.2.cloned.1.call-done = bf16[256,2048]{1,0:T(8,128)(2,1)} async-done(((bf16[256,2048]{1,0:T(8,128)(2,1)}), bf16[256,2048]{1,0:T(8,128)(2,1)}) %all-reduce.2.cloned.1.call-update) | async-done | bytes 1048592 | tf_op jit(solution)/shard_map/psum | solution.py:106
  165.4 2.0 fusion.25
  168.5 74.0 %all-gather.11.cloned.1.call-done = bf16[1024,2048]{1,0:T(8,128)(2,1)} async-done(((bf16[1024,256]{1,0:T(8,128)(2,1)}), bf16[1024,2048]{1,0:T(8,128)(2,1)}) %all-gather.11.cloned.1.call-update) | async-done | bytes 4194320 | tf_op jit(solution)/shard_map/all_gather | solution.py:119
  242.5 73.0 %all-gather.9.cloned.1.call-done = bf16[2048,1024]{1,0:T(8,128)(2,1)} async-done(((bf16[256,1024]{1,0:T(8,128)(2,1)}), bf16[2048,1024]{1,0:T(8,128)(2,1)}) %all-gather.9.cloned.1.call-update) | async-done | bytes 4194320 | tf_op jit(solution)/shard_map/all_gather | solution.py:116
  315.5 6.8 %convolution_convert_fusion = bf16[256,2048]{1,0:T(8,128)(2,1)} fusion(bf16[1024,2048]{1,0:T(8,128)(2,1)} %all-gather.11.cloned.1.call-done, bf16[256,2048]{1,0:T(8,128)(2,1)S(1)} %multiply_convert_fusion, bf16[2048,1024]{1,0:T(8,128)(2,1)} %all-gather.9.cloned.1.call-done), kind=kOutput, calls=%fused_computation.37 | convolution fusion | flops 2148794368 | bytes 10485760 | tf_op jit(solution)/shard_map/dot_general | solution.py:122
  322.3 23.5 %reduce-scatter.2.cloned.1.call-done = bf16[64,2048]{1,0:T(8,128)(2,1)} async-done(((bf16[256,2048]{1,0:T(8,128)(2,1)}), bf16[64,2048]{1,0:T(8,128)(2,1)}) %reduce-scatter.2.cloned.1.call-update) | async-done | bytes 262160 | tf_op jit(solution)/shard_map/reduce_scatter | solution.py:121
  345.8 1.7 add_convert_fusion
  (90 shorter events, 22.3 us)
Async XLA Ops:
  6.5 120.7 %copy-start = (bf16[256,2048]{1,0:T(8,128)(2,1)S(1)}, bf16[256,2048]{1,0:T(8,128)(2,1)}, u32[]{:S(2)}) copy-start(bf16[256,2048]{1,0:T(8,128)(2,1)} %param.22) | copy-start | bytes 3145732
  6.5 74.1 %all-gather.7.cloned.1.call-start = ((), (), s32[]{:S(2)}) async-start(), calls=%async_computation.2 | async-start | bytes 1179648 | tf_op jit(solution)/shard_map/all_gather | solution.py:76
  7.3 122.7 %all-gather.5.cloned.1.call-start = ((), (), s32[]{:S(2)}) async-start(), calls=%async_computation.1 | async-start | bytes 1310720 | tf_op jit(solution)/shard_map/all_gather | solution.py:109
  8.0 157.4 %all-reduce.2.cloned.1.call-start = ((), (), s32[]{:S(2)}) async-start(), calls=%async_computation.3 | async-start | bytes 2097152 | tf_op jit(solution)/shard_map/psum | solution.py:106
  86.3 4.7 %copy-start.3 = (f32[256,2]{0,1:T(2,128)S(1)}, f32[256,2]{0,1:T(2,128)}, u32[]{:S(2)}) copy-start(f32[256,2]{0,1:T(2,128)} %get-tuple-element.265) | copy-start | bytes 6148 | tf_op jit(solution)/shard_map/while
  96.2 4.9 %copy-start.3 = (f32[256,2]{0,1:T(2,128)S(1)}, f32[256,2]{0,1:T(2,128)}, u32[]{:S(2)}) copy-start(f32[256,2]{0,1:T(2,128)} %get-tuple-element.265) | copy-start | bytes 6148 | tf_op jit(solution)/shard_map/while
  107.3 4.9 %copy-start.3 = (f32[256,2]{0,1:T(2,128)S(1)}, f32[256,2]{0,1:T(2,128)}, u32[]{:S(2)}) copy-start(f32[256,2]{0,1:T(2,128)} %get-tuple-element.265) | copy-start | bytes 6148 | tf_op jit(solution)/shard_map/while
  118.4 4.9 %copy-start.3 = (f32[256,2]{0,1:T(2,128)S(1)}, f32[256,2]{0,1:T(2,128)}, u32[]{:S(2)}) copy-start(f32[256,2]{0,1:T(2,128)} %get-tuple-element.265) | copy-start | bytes 6148 | tf_op jit(solution)/shard_map/while
  128.7 113.7 %all-gather.11.cloned.1.call-start = ((), (), s32[]{:S(2)}) async-start(), calls=%async_computation.5 | async-start | bytes 4718592 | tf_op jit(solution)/shard_map/all_gather | solution.py:119
  129.3 186.1 %all-gather.9.cloned.1.call-start = ((), (), s32[]{:S(2)}) async-start(), calls=%async_computation.4 | async-start | bytes 4718592 | tf_op jit(solution)/shard_map/all_gather | solution.py:116
  129.4 38.6 %copy-start.4 = (f32[2048]{0:T(1024)S(1)}, f32[2048]{0:T(1024)}, u32[]{:S(2)}) copy-start(f32[2048]{0:T(1024)} %param.23) | copy-start | bytes 24580
  129.9 215.9 %reduce-scatter.2.cloned.1.call-start = ((), (), s32[]{:S(2)}) async-start(), calls=%async_computation.6 | async-start | bytes 1310720 | tf_op jit(solution)/shard_map/reduce_scatter | solution.py:121
  130.0 37.5 %copy-start.1 = (bf16[256,2048]{1,0:T(8,128)(2,1)S(1)}, bf16[256,2048]{1,0:T(8,128)(2,1)}, u32[]{:S(2)}) copy-start(bf16[256,2048]{1,0:T(8,128)(2,1)} %all-gather.5.cloned.1.call-done) | copy-start | bytes 3145732
  165.4 2.0 copy-start.2
Sparse Core Ops, SparseCore 0:
  9.5 45.4 all-gather.6
  56.5 15.4 all-gather.4
  128.9 36.5 all-reduce.1
  167.3 75.0 all-gather.10
  244.4 70.9 all-gather.8
  322.4 23.2 reduce-scatter.1
where the time goes:
time: 355 us; the launch traced here: 354 us
  waiting for transfers between devices  208 us (59%)
  blocking collectives  65.8 us (19%)
  matrix products  33 us (9%)
  local copies, waits for them, and re-layouts  20.2 us (6%)
  between operations  13.7 us (4%)
  other arithmetic  12.9 us (4%)
    all_gather x1, waiting for transfers between devices, local(): down_full = lax.all_gather(down_weight, 'sp', axis=1, tiled=True)  74 us
    all_gather x1, waiting for transfers between devices, local(): lax.all_gather(up_weight, 'sp', axis=0, tiled=True)  73 us
    psum x1, waiting for transfers between devices, local(): lax.psum(jnp.dot(flat, out_weight, preferred_element_type=jnp.float32).as...  35.5 us
    all_gather x1, blocking collectives, local(): piece_b = lax.all_gather(key_b, 'sp', axis=0, tiled=True)  34.2 us
    all_gather x1, blocking collectives, local(): piece_a = lax.all_gather(key_a, 'sp', axis=0, tiled=True)  31.6 us
    reduce_scatter x1, waiting for transfers between devices, local(): lax.psum_scatter(jnp.dot(hidden, down_full, preferred_element_type=jnp.fl...  23.5 us
    dot_general x8, matrix products, absorb(): jnp.einsum('qhk,khe->qhe', weights.astype(jnp.bfloat16), vals, preferred_...  14.6 us
    dynamic_slice x8, local copies, waits for them, and re-layouts, local(): state_a, state_b = lax.scan(advance, (start_state, start_state), items)[0]  11.8 us
  transfers between devices with their start and end apart: 6, of which 4 were waited for; matrix products, arithmetic and copies ran while one was open for 16% of the time, Pallas kernels for 0%

commit v1 on v0

--- a/solution.py
+++ b/solution.py
@@ -116,7 +116,7 @@
         lax.all_gather(up_weight, "sp", axis=0, tiled=True),
         preferred_element_type=jnp.float32,
     )
-    down_full = lax.all_gather(down_weight, "sp", axis=1, tiled=True)
+    down_full = jnp.concatenate(lax.all_gather(down_weight, "sp"), axis=1)
     hidden = jnp.square(jax.nn.relu(lifted)).astype(jnp.bfloat16)
     lowered = lax.psum_scatter(
         jnp.dot(hidden, down_full, preferred_element_type=jnp.float32).astype(jnp.bfloat16),

time: 355 us -> 354 us (level)
  waiting for transfers between devices: 208 us -> 201 us
  local copies, waits for them, and re-layouts: 20.2 us -> 26.7 us
    reshape x0 -> x1, local copies, waits for them, and re-layouts: none -> 6.48 us  [local(): down_full = jnp.concatenate(lax.all_gather(down_weight, 'sp'), axis=1)]
    all_gather x1, waiting for transfers between devices: 73 us -> 66.8 us  [local(): lax.all_gather(up_weight, 'sp', axis=0, tiled=True)]
  transfers between devices with their start and end apart: 6 -> 6, of which waited for: 4 -> 4; matrix products, arithmetic and copies ran while one was open for 16% -> 18% of each run, Pallas kernels for 0% -> 0%
where the time goes in v1:
time: 354 us; the launch traced here: 353 us
  waiting for transfers between devices  201 us (57%)
  blocking collectives  65.8 us (19%)
  matrix products  33 us (9%)
  local copies, waits for them, and re-layouts  26.7 us (8%)
  between operations  13.7 us (4%)
  other arithmetic  12.9 us (4%)
    all_gather x1, waiting for transfers between devices, local(): down_full = jnp.concatenate(lax.all_gather(down_weight, 'sp'), axis=1)  72.2 us
    all_gather x1, waiting for transfers between devices, local(): lax.all_gather(up_weight, 'sp', axis=0, tiled=True)  66.8 us
    psum x1, waiting for transfers between devices, local(): lax.psum(jnp.dot(flat, out_weight, preferred_element_type=jnp.float32).as...  35.6 us
    all_gather x1, blocking collectives, local(): piece_a = lax.all_gather(key_a, 'sp', axis=0, tiled=True)  34.2 us
    all_gather x1, blocking collectives, local(): piece_b = lax.all_gather(key_b, 'sp', axis=0, tiled=True)  31.6 us
    reduce_scatter x1, waiting for transfers between devices, local(): lax.psum_scatter(jnp.dot(hidden, down_full, preferred_element_type=jnp.fl...  23.5 us
    dot_general x8, matrix products, absorb(): jnp.einsum('qhk,khe->qhe', weights.astype(jnp.bfloat16), vals, preferred_...  14.6 us
    dynamic_slice x8, local copies, waits for them, and re-layouts, local(): state_a, state_b = lax.scan(advance, (start_state, start_state), items)[0]  11.8 us
  transfers between devices with their start and end apart: 6, of which 4 were waited for; matrix products, arithmetic and copies ran while one was open for 18% of the time, Pallas kernels for 0%

profile of v1, /device:TPU:0, one launch (start us, length us, event | category | flops | bytes accessed | tf_op | source)
XLA Modules:
  0.0 353.1 jit_solution(6376753761988505863)
XLA Ops:
  12.2 34.2 %all_gather.22 = bf16[2048,128]{0,1:T(8,128)(2,1)S(1)} all-gather(bf16[256,128]{0,1:T(8,128)(2,1)S(1)} %bitcast.72), channel_id=1, replica_groups=mesh['sp'=8,'tp'=4] {'sp'}, dimensions={0}, use_global_device_ids=true | all-gather | bytes 589824 | tf_op jit(solution)/shard_map/all_gather | solution.py:74
  47.7 31.6 %all_gather.24 = bf16[2048,128]{0,1:T(8,128)(2,1)S(1)} all-gather(bf16[256,128]{0,1:T(8,128)(2,1)S(1)} %bitcast.73), channel_id=1, replica_groups=mesh['sp'=8,'tp'=4] {'sp'}, dimensions={0}, use_global_device_ids=true | all-gather | bytes 589824 | tf_op jit(solution)/shard_map/all_gather | solution.py:75
  80.6 2.1 reshape.140
  82.7 42.6 %while.21 = (s32[]{:T(128)}, f32[256,2]{0,1:T(2,128)S(1)}, f32[256,2]{0,1:T(2,128)}, f32[256,2,128]{0,2,1:T(8,128)}, f32[256,2]{0,1:T(2,128)S(1)}, /*index=5*/f3...) while((s32[]{:T(128)}, f32[256,2]{0,1:T(2,128)S(1)}, ...), condition=%wide.region_5.6_spmd.clone, body=%wide.region_0.5_spmd.clone.sunk | while | flops 204870656 | bytes 9381043 | solution.py:96
  82.7 1.3 fusion.60
  84.2 1.3 fusion.62
  86.3 1.8 constant_dynamic-slice_fusion.2
  89.2 1.7 fusion.68
  93.4 1.3 fusion.62
  94.8 1.3 fusion.66
  96.2 1.8 constant_dynamic-slice_fusion.2
  99.1 2.0 fusion.68
  101.1 2.0 fusion.67
  104.5 1.3 fusion.62
  106.0 1.3 fusion.66
  107.3 1.8 constant_dynamic-slice_fusion.2
  110.2 2.0 fusion.68
  112.2 2.0 fusion.67
  115.6 1.3 fusion.62
  117.1 1.3 fusion.66
  118.4 1.8 constant_dynamic-slice_fusion.2
  121.4 2.0 fusion.68
  123.4 2.0 fusion.67
  127.3 1.4 convolution_convert_fusion.1
  130.0 35.6 %all-reduce.2.cloned.1.call-done = bf16[256,2048]{1,0:T(8,128)(2,1)} async-done(((bf16[256,2048]{1,0:T(8,128)(2,1)}), bf16[256,2048]{1,0:T(8,128)(2,1)}) %all-reduce.2.cloned.1.call-update) | async-done | bytes 1048592 | tf_op jit(solution)/shard_map/psum | solution.py:106
  165.6 2.0 fusion.25
  168.6 72.2 %all-gather.12.cloned.1.call-done = bf16[8192,256]{1,0:T(8,128)(2,1)} async-done(((bf16[1024,256]{1,0:T(8,128)(2,1)}), bf16[8192,256]{1,0:T(8,128)(2,1)}) %all-gather.12.cloned.1.call-update) | async-done | bytes 4194320 | tf_op jit(solution)/shard_map/all_gather | solution.py:119
  240.9 6.5 %copy.37 = bf16[1024,8,256]{0,2,1:T(8,128)(2,1)} copy(bf16[1024,8,256]{2,0,1:T(8,128)(2,1)} %bitcast.65) | data formatting | bytes 8388608 | tf_op jit(solution)/shard_map/reshape | solution.py:119
  247.4 66.8 %all-gather.10.cloned.1.call-done = bf16[2048,1024]{1,0:T(8,128)(2,1)} async-done(((bf16[256,1024]{1,0:T(8,128)(2,1)}), bf16[2048,1024]{1,0:T(8,128)(2,1)}) %all-gather.10.cloned.1.call-update) | async-done | bytes 4194320 | tf_op jit(solution)/shard_map/all_gather | solution.py:116
  314.2 6.8 %convolution_convert_fusion = bf16[256,2048]{1,0:T(8,128)(2,1)} fusion(bf16[1024,2048]{0,1:T(8,128)(2,1)} %bitcast.66, bf16[256,2048]{1,0:T(8,128)(2,1)S(1)} %multiply_convert_fusion, bf16[2048,1024]{1,0:T(8,128)(2,1)} %all-gather.10.cloned.1.call-done), kind=kOutput, calls=%fused_computation.37 | convolution fusion | flops 2148794368 | bytes 10485760 | tf_op jit(solution)/shard_map/dot_general | solution.py:122
  321.0 23.5 %reduce-scatter.2.cloned.1.call-done = bf16[64,2048]{1,0:T(8,128)(2,1)} async-done(((bf16[256,2048]{1,0:T(8,128)(2,1)}), bf16[64,2048]{1,0:T(8,128)(2,1)}) %reduce-scatter.2.cloned.1.call-update) | async-done | bytes 262160 | tf_op jit(solution)/shard_map/reduce_scatter | solution.py:121
  344.5 1.7 add_convert_fusion
  (91 shorter events, 23.5 us)
Async XLA Ops:
  6.5 120.7 %copy-start = (bf16[256,2048]{1,0:T(8,128)(2,1)S(1)}, bf16[256,2048]{1,0:T(8,128)(2,1)}, u32[]{:S(2)}) copy-start(bf16[256,2048]{1,0:T(8,128)(2,1)} %param.22) | copy-start | bytes 3145732
  6.5 74.1 %all-gather.8.cloned.1.call-start = ((), (), s32[]{:S(2)}) async-start(), calls=%async_computation.2 | async-start | bytes 1179648 | tf_op jit(solution)/shard_map/all_gather | solution.py:76
  7.3 122.7 %all-gather.6.cloned.1.call-start = ((), (), s32[]{:S(2)}) async-start(), calls=%async_computation.1 | async-start | bytes 1310720 | tf_op jit(solution)/shard_map/all_gather | solution.py:109
  8.0 157.6 %all-reduce.2.cloned.1.call-start = ((), (), s32[]{:S(2)}) async-start(), calls=%async_computation.3 | async-start | bytes 2097152 | tf_op jit(solution)/shard_map/psum | solution.py:106
  86.3 4.7 %copy-start.3 = (f32[256,2]{0,1:T(2,128)S(1)}, f32[256,2]{0,1:T(2,128)}, u32[]{:S(2)}) copy-start(f32[256,2]{0,1:T(2,128)} %get-tuple-element.277) | copy-start | bytes 6148 | tf_op jit(solution)/shard_map/while
  96.2 4.9 %copy-start.3 = (f32[256,2]{0,1:T(2,128)S(1)}, f32[256,2]{0,1:T(2,128)}, u32[]{:S(2)}) copy-start(f32[256,2]{0,1:T(2,128)} %get-tuple-element.277) | copy-start | bytes 6148 | tf_op jit(solution)/shard_map/while
  107.3 4.9 %copy-start.3 = (f32[256,2]{0,1:T(2,128)S(1)}, f32[256,2]{0,1:T(2,128)}, u32[]{:S(2)}) copy-start(f32[256,2]{0,1:T(2,128)} %get-tuple-element.277) | copy-start | bytes 6148 | tf_op jit(solution)/shard_map/while
  118.4 4.9 %copy-start.3 = (f32[256,2]{0,1:T(2,128)S(1)}, f32[256,2]{0,1:T(2,128)}, u32[]{:S(2)}) copy-start(f32[256,2]{0,1:T(2,128)} %get-tuple-element.277) | copy-start | bytes 6148 | tf_op jit(solution)/shard_map/while
  128.7 112.1 %all-gather.12.cloned.1.call-start = ((), (), s32[]{:S(2)}) async-start(), calls=%async_computation.6 | async-start | bytes 4718592 | tf_op jit(solution)/shard_map/all_gather | solution.py:119
  129.3 184.9 %all-gather.10.cloned.1.call-start = ((), (), s32[]{:S(2)}) async-start(), calls=%async_computation.4 | async-start | bytes 4718592 | tf_op jit(solution)/shard_map/all_gather | solution.py:116
  129.4 38.8 %copy-start.4 = (f32[2048]{0:T(1024)S(1)}, f32[2048]{0:T(1024)}, u32[]{:S(2)}) copy-start(f32[2048]{0:T(1024)} %param.23) | copy-start | bytes 24580
  129.9 214.6 %reduce-scatter.2.cloned.1.call-start = ((), (), s32[]{:S(2)}) async-start(), calls=%async_computation.5 | async-start | bytes 1310720 | tf_op jit(solution)/shard_map/reduce_scatter | solution.py:121
  130.0 37.6 %copy-start.1 = (bf16[256,2048]{1,0:T(8,128)(2,1)S(1)}, bf16[256,2048]{1,0:T(8,128)(2,1)}, u32[]{:S(2)}) copy-start(bf16[256,2048]{1,0:T(8,128)(2,1)} %all-gather.6.cloned.1.call-done) | copy-start | bytes 3145732
  165.6 2.0 copy-start.2
Sparse Core Ops, SparseCore 0:
  9.5 45.4 all-gather.7
  56.5 15.4 all-gather.5
  128.9 36.7 all-reduce.1
  167.6 73.2 all-gather.11
  242.8 71.3 all-gather.9
  321.1 23.3 reduce-scatter.1
